TPU v7x, 32 devices: a whole 2x2x4 slice. The times are simulated.
32 devices in a mesh: ep: 8 (over z, x), tp: 4 (over y, core).
Axes of the slice: x: 2, y: 2, z: 4, core: 2. Of those that a mesh axis runs over, the one named last changes fastest.
Arguments:
- mix_query: bfloat16 [2048, 2048], P('ep', 'tp'), may hold values from -6 to 6
- forget_input: bfloat16 [2048, 2048], P('ep', 'tp'), may hold values from -6 to 6
- mix_value: bfloat16 [2048, 2048], P('ep', 'tp'), may hold values from -6 to 6
- out_gate_input: bfloat16 [2048, 2048], P('ep', 'tp'), may hold values from -6 to 6
- decay_shift: float32 [2048, 16], P('ep', 'tp'), may hold values from -1.5 to 0
- forget_floor: float32 [2048], P('tp'), may hold values from 0.9 to 1
- head_gain: float32 [128], replicated, may hold values from 0.1 to 1.9
- w_mix_out: bfloat16 [2048, 2048], P(None, 'tp'), may hold values from -0.125 to 0.125
- moe_input: bfloat16 [2048, 2048], P('ep'), may hold values from -6 to 6
- moe_gain: float32 [2048], replicated, may hold values from 0.1 to 1.9
- routes: int32 [2048, 2], P('ep'), may hold values from 0 to 7, all different within a row; in each aligned block of 256 rows (0 to 255, 256 to 511, ...) at most 80 rows name the same one
- route_weight: float32 [2048, 2], P('ep'), may hold values from 0.1 to 1
- w_exp_gate: bfloat16 [8, 2048, 4096], P('ep', None, 'tp'), may hold values from -0.125 to 0.125
- w_exp_up: bfloat16 [8, 2048, 4096], P('ep', None, 'tp'), may hold values from -0.125 to 0.125
- w_exp_down: bfloat16 [8, 4096, 2048], P('ep', 'tp'), may hold values from -0.125 to 0.125
Outputs:
- mixed: bfloat16 [2048, 2048], P('ep', 'tp')
- moe_out: bfloat16 [2048, 2048], P('ep', 'tp')
Inputs may be any that keep to these rules, and one draw needn't show every extreme that they name: `routes`: at most 80 of the rows of one index of ep name one expert, and in every draw some device's rows name one expert exactly 80 times; the experts of a row differ.
All inputs are finite; a program needn't handle non-finite values.
Results may differ from a plain program's by a relative error of at most 0.02.
Values may be sent and summed in bfloat16 or wider, within the bound.
A program may use at most 64 MiB of HBM per device.

v0:
```python
import jax
import jax.numpy as jnp
from jax import lax
from jax.sharding import PartitionSpec as P

TOP_K = 2
eps = 1e-06
highest_precision = lax.Precision.HIGHEST


def carried_in(shard, axis, join, neutral):
    place = lax.axis_index(axis)
    gathered = jax.tree.map(
        lambda a, kind: lax.all_gather(a.astype(kind), axis), shard, (jnp.bfloat16, jnp.bfloat16)
    )
    state = jax.tree.map(lambda a, e: jnp.zeros_like(a) + jnp.asarray(e, a.dtype), shard, neutral)

    def one(turn, state):
        return join(
            state,
            jax.tree.map(
                lambda a, own: lax.dynamic_index_in_dim(a, turn, 0, False).astype(own.dtype),
                gathered,
                shard,
            ),
        )

    return lax.fori_loop(0, place, one, state)


def chain_step(earlier, later):
    return (earlier[0] * later[0], later[0][:, :, None] * earlier[1] + later[1])


def token_mixer(
    mix_query,
    forget_input,
    mix_value,
    out_gate_input,
    decay_shift,
    forget_floor,
    head_gain,
    w_mix_out,
):
    length = mix_query.shape[0]
    heads_here = decay_shift.shape[1]
    head_size = head_gain.shape[0]
    gate_input = forget_input.astype(jnp.float32)
    forget = forget_floor + (1.0 - forget_floor) * jax.nn.sigmoid(gate_input)
    input_gate = (1.0 - forget_floor) * jax.nn.sigmoid(-gate_input)
    log_decay = jnp.log(forget) + jnp.repeat(decay_shift, head_size, axis=1)

    def by_head(array):
        return array.reshape(length, heads_here, head_size).transpose(1, 0, 2)

    running_decay = jnp.cumsum(by_head(log_decay), axis=1)
    query_rows = by_head(mix_query.astype(jnp.float32)) * jnp.exp(running_decay)
    head_keys = by_head(input_gate)
    values = by_head(mix_value.astype(jnp.float32))
    scores = jnp.einsum(
        "htk,hsk->hts", query_rows, head_keys * jnp.exp(-running_decay), precision=highest_precision
    )
    causal = jnp.arange(length)[:, None] >= jnp.arange(length)[None, :]
    scores = jnp.where(causal[None, :, :], scores, 0.0)
    within_block_output = jnp.einsum("hts,hsv->htv", scores, values, precision=highest_precision)
    closing_total = running_decay[:, -1, :]
    carried_over_state = jnp.einsum(
        "gbx,gbi->gxi",
        head_keys * jnp.exp(closing_total[:, None, :] - running_decay),
        values,
        precision=highest_precision,
    )
    incoming_state = carried_in(
        (jnp.exp(closing_total), carried_over_state),
        "ep",
        chain_step,
        (jnp.ones_like(closing_total), jnp.zeros_like(carried_over_state)),
    )[1]
    block_result = within_block_output + jnp.einsum(
        "rsd,rda->rsa", query_rows, incoming_state, precision=highest_precision
    )
    inverse = lax.rsqrt(jnp.mean(block_result * block_result, axis=2, keepdims=True) + eps)
    gated = by_head(jax.nn.silu(out_gate_input.astype(jnp.float32)))
    normed_heads = (block_result * inverse * head_gain * gated).transpose(1, 0, 2)
    head_out = normed_heads.reshape(length, heads_here * head_size).astype(jnp.bfloat16)
    mixed = jnp.dot(
        lax.all_gather(head_out, "tp", axis=1, tiled=True),
        w_mix_out,
        preferred_element_type=jnp.float32,
    )
    return mixed.astype(jnp.bfloat16)


def experts_layer(moe_input, moe_gain, routes, route_weight, w_exp_gate, w_exp_up, w_exp_down):
    row_count = moe_input.shape[0]
    expert_count = lax.axis_size("ep")
    capacity = 5 * row_count * TOP_K // (4 * expert_count)
    token_rows = moe_input.astype(jnp.float32)
    inverse = lax.rsqrt(jnp.mean(token_rows * token_rows, axis=1, keepdims=True) + eps)
    normed = (token_rows * inverse * moe_gain).astype(jnp.bfloat16)
    flat_ids = routes.reshape(-1)
    pair_count = flat_ids.shape[0]
    one_hot = (flat_ids[:, None] == jnp.arange(expert_count, dtype=jnp.int32)[None, :]).astype(
        jnp.int32
    )
    earlier_count = jnp.cumsum(one_hot, axis=0) - one_hot
    ranks = jnp.sum(earlier_count * one_hot, axis=1)
    slot_ids = flat_ids * capacity + ranks
    owners = (
        jnp.zeros((expert_count * capacity,), jnp.int32)
        .at[slot_ids]
        .set(jnp.arange(pair_count, dtype=jnp.int32) // TOP_K)
    )
    filled = (
        jnp.zeros((expert_count * capacity,), jnp.bfloat16)
        .at[slot_ids]
        .set(jnp.ones((pair_count,), jnp.bfloat16))
    )
    outgoing = normed[owners] * filled[:, None]
    w_gate = w_exp_gate[0]
    w_up = w_exp_up[0]
    w_down = w_exp_down[0]
    width = normed.shape[1] // lax.axis_size("tp")
    own_slice = lax.dynamic_slice_in_dim(outgoing, lax.axis_index("tp") * width, width, 1)
    arrived = lax.all_to_all(own_slice, "ep", split_axis=0, concat_axis=0, tiled=True)
    portion = lax.all_gather(arrived, "tp", axis=1, tiled=True)
    gate_sum = jnp.dot(portion, w_gate, preferred_element_type=jnp.float32)
    up_sum = jnp.dot(portion, w_up, preferred_element_type=jnp.float32)
    hidden = (jax.nn.silu(gate_sum) * up_sum).astype(jnp.bfloat16)
    partial_value = jnp.dot(hidden, w_down, preferred_element_type=jnp.float32)
    summed = lax.psum_scatter(
        partial_value.astype(jnp.bfloat16), "tp", scatter_dimension=1, tiled=True
    )
    returned = lax.all_to_all(summed, "ep", split_axis=0, concat_axis=0, tiled=True)
    picked = returned[slot_ids].astype(jnp.float32).reshape(row_count, TOP_K, returned.shape[1])
    combined = jnp.sum(picked * route_weight[:, :, None], axis=1)
    return combined.astype(jnp.bfloat16)


def body(
    mix_query,
    forget_input,
    mix_value,
    out_gate_input,
    decay_shift,
    forget_floor,
    head_gain,
    w_mix_out,
    moe_input,
    moe_gain,
    routes,
    route_weight,
    w_exp_gate,
    w_exp_up,
    w_exp_down,
):
    mixed = token_mixer(
        mix_query,
        forget_input,
        mix_value,
        out_gate_input,
        decay_shift,
        forget_floor,
        head_gain,
        w_mix_out,
    )
    moe_out = experts_layer(
        moe_input, moe_gain, routes, route_weight, w_exp_gate, w_exp_up, w_exp_down
    )
    return (mixed, moe_out)


def solution(mesh):
    placed = (
        P("ep", "tp"),
        P("ep", "tp"),
        P("ep", "tp"),
        P("ep", "tp"),
        P("ep", "tp"),
        P("tp"),
        P(),
        P(None, "tp"),
        P("ep", None),
        P(),
        P("ep", None),
        P("ep", None),
        P("ep", None, "tp"),
        P("ep", None, "tp"),
        P("ep", "tp", None),
    )
    return jax.shard_map(
        body, mesh=mesh, in_specs=placed, out_specs=(P("ep", "tp"), P("ep", "tp")), check_vma=False
    )
```

profile of v0, /device:TPU:0, one launch (start us, length us, event | category | flops | bytes accessed | tf_op | source)
XLA Modules:
  0.0 189.2 jit_solution(8927491651452208620)
XLA Ops:
  11.0 2.4 %scatter_custom_fusion = s32[640]{0:T(1024)S(1)} fusion(s32[512]{0:T(512)S(1)} %bitcast.123, s32[512]{0:T(512)S(1)} %add_select_fusion, s32[]{:T(128)} %constant.68.clone.1), kind=kCustom, calls=%fused_computation.82 | custom fusion | bytes 2564 | tf_op jit(solution)/shard_map/scatter | solution.py:112
  13.5 1.5 fusion.9
  15.0 1.5 fusion.11
  16.5 4.1 %gather_fusion = bf16[640,2048]{1,0:T(8,128)(2,1)} fusion(bf16[256,2048]{1,0:T(8,128)(2,1)S(1)} %fusion.11, s32[1024]{0:T(1024)S(1)} %pad_clamp_fusion.1), kind=kCustom, calls=%fused_computation | custom fusion | bytes 5245440 | tf_op jit(solution)/shard_map/gather | solution.py:119
  20.6 3.8 %scatter_custom_fusion.1 = bf16[640]{0:T(1024)(128)(2,1)S(1)} fusion(s32[512]{0:T(512)S(1)} %bitcast.124, bf16[512]{0:T(512)(128)(2,1)S(1)} %broadcast.119, bf16[]{:T(256)} %constant.79.clone.1), kind=kCustom, calls=%fused_computation.87 | custom fusion | bytes 1282 | tf_op jit(solution)/shard_map/scatter | solution.py:117
  24.4 1.3 dynamic-slice_multiply_fusion
  25.7 24.9 %all_to_all.24 = bf16[8,80,512]{2,1,0:T(8,128)(2,1)} all-to-all(bf16[8,80,512]{2,1,0:T(8,128)(2,1)S(1)} %bitcast.112), channel_id=1, replica_groups=mesh['ep'=8,'tp'=4] {'ep'}, dimensions={0} | all-to-all | bytes 1310720 | tf_op jit(solution)/shard_map/all_to_all | solution.py:125
  53.9 2.2 %copy.97 = f32[256,4,128]{2,1,0:T(4,128)} copy(f32[256,4,128]{0,2,1:T(8,128)} %bitcast.114) | data formatting | bytes 1048576 | tf_op jit(solution)/shard_map/reshape | solution.py:54
  58.8 2.8 %bitcast_multiply_fusion.2 = (f32[4,256,128]{2,0,1:T(4,128)}, f32[4,256,128]{2,0,1:T(4,128)S(1)}, f32[4,256,128]{2,0,1:T(4,128)S(1)}) fusion(f32[256,4,128]{2,1,0:T(4,128)} %copy.97, f32[4,128,256]{1,2,0:T(8,128)S(1)} %bitcast.110, f32[4,128]{1,0:T(4,128)S(1)} %get-tuple-element.60, f32[256,4,128]{2,1,0:T(4,128)} %copy.91), kind=kLoop, calls=%fused_computation.47 | loop fusion | flops 655360 | bytes 3147776 | tf_op jit(solution)/shard_map/mul | solution.py:61
  61.5 1.3 convolution_convert_fusion.1
  63.1 11.9 %all-gather.8.cloned.1.call-done = bf16[640,2048]{1,0:T(8,128)(2,1)} async-done(((bf16[640,512]{1,0:T(8,128)(2,1)}), bf16[640,2048]{1,0:T(8,128)(2,1)}) %all-gather.8.cloned.1.call-update) | async-done | bytes 2621456 | tf_op jit(solution)/shard_map/all_gather | solution.py:126
  75.0 7.4 %fusion.2 = f32[640,1024]{1,0:T(8,128)} fusion(bf16[640,2048]{1,0:T(8,128)(2,1)} %all-gather.8.cloned.1.call-done, bf16[1,2048,1024]{2,1,0:T(8,128)(2,1)} %param.30), kind=kOutput, calls=%fused_computation.8 | convolution fusion | flops 2684354560 | bytes 9437184 | tf_op jit(solution)/shard_map/dot_general | solution.py:128
  82.3 12.5 %fusion.6 = bf16[640,2048]{1,0:T(8,128)(2,1)} fusion(bf16[1,1024,2048]{2,1,0:T(8,128)(2,1)} %param.31, f32[640,1024]{1,0:T(8,128)} %fusion.2, bf16[640,2048]{1,0:T(8,128)(2,1)} %all-gather.8.cloned.1.call-done, bf16[1,2048,1024]{2,1,0:T(8,128)(2,1)} %param.29), kind=kOutput, calls=%fused_computation.12 | convolution fusion | flops 5373952000 | bytes 16252928 | tf_op jit(solution)/shard_map/dot_general | solution.py:130
  94.9 26.4 %all-gather = bf16[32,1,128]{2,1,0:T(2,128)(2,1)S(1)} all-gather(bf16[4,1,128]{2,1,0:T(2,128)(2,1)S(1)} %copy.102), channel_id=2, replica_groups=mesh['ep'=8,'tp'=4] {'ep'}, dimensions={0}, use_global_device_ids=true | all-gather | bytes 9216 | tf_op jit(solution)/shard_map/all_gather | solution.py:14
  121.6 3.0 %convolution_select_fusion = f32[4,256,256]{2,1,0:T(8,128)} fusion(f32[4,256,128]{2,0,1:T(4,128)} %get-tuple-element.57, pred[256,256]{1,0:T(8,128)(4,1)S(1)} %iota_compare_fusion, f32[4,256,128]{2,0,1:T(4,128)S(1)} %get-tuple-element.59), kind=kOutput, calls=%fused_computation.19 | convolution fusion | flops 402915328 | bytes 2162688 | tf_op jit(solution)/shard_map/htk,hsk->hts/dot_general | solution.py:60
  125.4 2.2 %multiply_reduce_fusion.1 = (f32[4,256]{1,0:T(4,128)S(1)}, f32[4,256,128]{1,2,0:T(8,128)S(1)}) fusion(f32[4,256,128]{1,2,0:T(8,128)S(1)} %fusion.36, f32[4,256,256]{2,1,0:T(8,128)} %convolution_select_fusion, bf16[256,512]{1,0:T(8,128)(2,1)} %param.19), kind=kOutput, calls=%fused_computation.54 | convolution fusion | flops 403045376 | bytes 2363392 | tf_op jit(solution)/shard_map/hts,hsv->htv/dot_general | solution.py:65
  128.4 25.2 %reduce-scatter.2.cloned.1.call-done = bf16[640,512]{1,0:T(8,128)(2,1)} async-done(((bf16[640,2048]{1,0:T(8,128)(2,1)}), bf16[640,512]{1,0:T(8,128)(2,1)}) %reduce-scatter.2.cloned.1.call-update) | async-done | bytes 655376 | tf_op jit(solution)/shard_map/reduce_scatter | solution.py:131
  153.7 5.5 %all-to-all-start.1 = ((bf16[8,80,512]{2,1,0:T(8,128)(2,1)}), bf16[8,80,512]{2,1,0:T(8,128)(2,1)S(1)}, u32[]{:S(2)}, u32[]{:S(2)}) async-start(bf16[8,80,512]{2,1,0:T(8,128)(2,1)} %bitcast.119), calls=%async_computation.2 | async-start | bytes 1310720 | tf_op jit(solution)/shard_map/all_to_all | solution.py:134
  159.3 13.1 %all-gather.6.cloned.1.call-done = bf16[256,2048]{0,1:T(8,128)(2,1)} async-done(((bf16[256,512]{0,1:T(8,128)(2,1)}), bf16[256,2048]{0,1:T(8,128)(2,1)}) %all-gather.6.cloned.1.call-update) | async-done | bytes 1048592 | tf_op jit(solution)/shard_map/all_gather | solution.py:87
  172.4 2.7 %convolution_convert_fusion = bf16[256,512]{1,0:T(8,128)(2,1)} fusion(bf16[256,2048]{0,1:T(8,128)(2,1)} %all-gather.6.cloned.1.call-done, bf16[2048,512]{1,0:T(8,128)(2,1)S(1)} %copy-done), kind=kOutput, calls=%fused_computation.21 | convolution fusion | flops 537001984 | bytes 3407872 | tf_op jit(solution)/shard_map/dot_general | solution.py:86
  175.0 1.3 all-to-all-done.1
  176.3 2.6 %gather_fusion.1 = bf16[512,512]{1,0:T(8,128)(2,1)} fusion(bf16[640,512]{1,0:T(8,128)(2,1)S(1)} %bitcast.108, s32[1024]{0:T(1024)S(1)} %pad_clamp_fusion), kind=kCustom, calls=%fused_computation.1 | custom fusion | bytes 1050624 | tf_op jit(solution)/shard_map/gather | solution.py:135
  178.9 1.7 reshape.158
  180.6 2.1 %multiply_reduce_fusion = bf16[256,512]{1,0:T(8,128)(2,1)} fusion(f32[256,2,512]{2,1,0:T(2,128)S(1)} %reshape.158, f32[256,2]{1,0:T(8,128)S(1)} %copy.110), kind=kLoop, calls=%fused_computation.23 | loop fusion | flops 393216 | bytes 1312768 | tf_op jit(solution)/shard_map/reduce_sum | solution.py:136
  (69 shorter events, 12.1 us)
Async XLA Ops:
  7.2 165.2 %copy-start = (bf16[2048,512]{1,0:T(8,128)(2,1)S(1)}, bf16[2048,512]{1,0:T(8,128)(2,1)}, u32[]{:S(2)}) copy-start(bf16[2048,512]{1,0:T(8,128)(2,1)} %param.24) | copy-start | bytes 6291460
  7.2 67.8 %all-gather.8.cloned.1.call-start = ((), (), s32[]{:S(2)}) async-start(), calls=%async_computation.4 | async-start | bytes 3276800 | tf_op jit(solution)/shard_map/all_gather | solution.py:126
  20.6 30.0 %copy-start.2 = (bf16[256,512]{1,0:T(8,128)(2,1)S(1)}, bf16[256,512]{1,0:T(8,128)(2,1)}, u32[]{:S(2)}) copy-start(bf16[256,512]{1,0:T(8,128)(2,1)} %param.18) | copy-start | bytes 786436
  20.6 30.2 %copy-start.4 = (f32[512]{0:T(512)S(1)}, f32[512]{0:T(512)}, u32[]{:S(2)}) copy-start(f32[512]{0:T(512)} %param.22) | copy-start | bytes 6148
  20.6 30.2 %copy-start.5 = (f32[256,4]{0,1:T(4,128)S(1)}, f32[256,4]{0,1:T(4,128)}, u32[]{:S(2)}) copy-start(f32[256,4]{0,1:T(4,128)} %param.21) | copy-start | bytes 12292
  50.6 74.1 %all-gather.10.cloned.1.call-start = ((), (), s32[]{:S(2)}) async-start(), calls=%async_computation.6 | async-start | bytes 1179648 | tf_op jit(solution)/shard_map/all_gather | solution.py:14
  53.9 7.6 %copy-start.1 = (bf16[256,512]{1,0:T(8,128)(2,1)S(1)}, bf16[256,512]{1,0:T(8,128)(2,1)}, u32[]{:S(2)}) copy-start(bf16[256,512]{1,0:T(8,128)(2,1)} %param.19) | copy-start | bytes 786436
  62.9 90.8 %reduce-scatter.2.cloned.1.call-start = ((), (), s32[]{:S(2)}) async-start(), calls=%async_computation.5 | async-start | bytes 3276800 | tf_op jit(solution)/shard_map/reduce_scatter | solution.py:131
  94.8 26.5 %copy-start.3 = (bf16[256,512]{1,0:T(8,128)(2,1)S(1)}, bf16[256,512]{1,0:T(8,128)(2,1)}, u32[]{:S(2)}) copy-start(bf16[256,512]{1,0:T(8,128)(2,1)} %param.20) | copy-start | bytes 786436
  94.8 77.6 %all-gather.6.cloned.1.call-start = ((), (), s32[]{:S(2)}) async-start(), calls=%async_computation.3 | async-start | bytes 1310720 | tf_op jit(solution)/shard_map/all_gather | solution.py:87
  124.7 2.9 %copy-start.7 = (f32[128]{0:T(128)S(1)}, f32[128]{0:T(128)}, u32[]{:S(2)}) copy-start(f32[128]{0:T(128)} %param.23) | copy-start | bytes 1540
  125.4 33.8 %copy-start.6 = (f32[256,2]{0,1:T(2,128)S(1)}, f32[256,2]{0,1:T(2,128)}, u32[]{:S(2)}) copy-start(f32[256,2]{0,1:T(2,128)} %param.28) | copy-start | bytes 6148
  153.7 22.6 %all-to-all-start.1 = ((bf16[8,80,512]{2,1,0:T(8,128)(2,1)}), bf16[8,80,512]{2,1,0:T(8,128)(2,1)S(1)}, u32[]{:S(2)}, u32[]{:S(2)}) async-start(bf16[8,80,512]{2,1,0:T(8,128)(2,1)} %bitcast.119), calls=%async_computation.2 | async-start | bytes 1310720 | tf_op jit(solution)/shard_map/all_to_all | solution.py:134
Sparse Core Ops, SparseCore 0:
  50.7 24.2 all-gather.7
  77.7 40.3 all-gather.9
  120.5 33.0 reduce-scatter.1
  155.7 16.6 all-gather.5
where the time goes:
time: 190 us; the launch traced here: 189 us
  waiting for transfers between devices  51.5 us (27%)
  blocking collectives  51.3 us (27%)
  matrix products  29.7 us (16%)
  local copies, waits for them, and re-layouts  22.4 us (12%)
  other arithmetic  14.5 us (8%)
  between operations  14 us (7%)
  starting transfers between devices  5.83 us (3%)
    all_gather x1, blocking collectives, carried_in(): lax.all_gather(a.astype(kind), axis)  26.4 us
    reduce_scatter x1, waiting for transfers between devices, experts_layer(): lax.psum_scatter(partial_value.astype(jnp.bfloat16), 'tp', scatter_dimens...  25.2 us
    all_to_all x1, blocking collectives, experts_layer(): lax.all_to_all(own_slice, 'ep', split_axis=0, concat_axis=0, tiled=True)  24.9 us
    all_gather x1, waiting for transfers between devices, token_mixer(): lax.all_gather(head_out, 'tp', axis=1, tiled=True)  13.1 us
    dot_general x1, matrix products, experts_layer(): partial_value = jnp.dot(hidden, w_down, preferred_element_type=jnp.float32)  12.5 us
    all_gather x1, waiting for transfers between devices, experts_layer(): portion = lax.all_gather(arrived, 'tp', axis=1, tiled=True)  11.9 us
    dot_general x1, matrix products, experts_layer(): up_sum = jnp.dot(portion, w_up, preferred_element_type=jnp.float32)  7.36 us
    all_to_all x1, starting transfers between devices, experts_layer(): lax.all_to_all(summed, 'ep', split_axis=0, concat_axis=0, tiled=True)  5.49 us
  transfers between devices with their start and end apart: 5, of which 4 were waited for; matrix products, arithmetic and copies ran while one was open for 22% of the time, Pallas kernels for 0%

commit v1 on v0

--- a/solution.py
+++ b/solution.py
@@ -84,7 +84,7 @@
     normed_heads = (block_result * inverse * head_gain * gated).transpose(1, 0, 2)
     head_out = normed_heads.reshape(length, heads_here * head_size).astype(jnp.bfloat16)
     mixed = jnp.dot(
-        lax.all_gather(head_out, "tp", axis=1, tiled=True),
+        jnp.concatenate(lax.all_gather(head_out, "tp"), axis=1),
         w_mix_out,
         preferred_element_type=jnp.float32,
     )

time: 190 us -> 191 us (level)
  local copies, waits for them, and re-layouts: 22.4 us -> 25.5 us
    all_gather x0 -> x1, local copies, waits for them, and re-layouts: none -> 2.28 us  [token_mixer(): lax.all_gather(head_out, 'tp')]
  transfers between devices with their start and end apart: 5 -> 5, of which waited for: 4 -> 3; matrix products, arithmetic and copies ran while one was open for 22% -> 23% of each run, Pallas kernels for 0% -> 0%
where the time goes in v1:
time: 191 us; the launch traced here: 190 us
  blocking collectives  51.3 us (27%)
  waiting for transfers between devices  50.1 us (26%)
  matrix products  29.7 us (16%)
  local copies, waits for them, and re-layouts  25.5 us (13%)
  between operations  14.1 us (7%)
  other arithmetic  13.8 us (7%)
  starting transfers between devices  5.83 us (3%)
    all_gather x1, blocking collectives, carried_in(): lax.all_gather(a.astype(kind), axis)  26.4 us
    reduce_scatter x1, waiting for transfers between devices, experts_layer(): lax.psum_scatter(partial_value.astype(jnp.bfloat16), 'tp', scatter_dimens...  25.1 us
    all_to_all x1, blocking collectives, experts_layer(): lax.all_to_all(own_slice, 'ep', split_axis=0, concat_axis=0, tiled=True)  24.9 us
    all_gather x1, waiting for transfers between devices, token_mixer(): lax.all_gather(head_out, 'tp')  13.1 us
    dot_general x1, matrix products, experts_layer(): partial_value = jnp.dot(hidden, w_down, preferred_element_type=jnp.float32)  12.5 us
    all_gather x1, waiting for transfers between devices, experts_layer(): portion = lax.all_gather(arrived, 'tp', axis=1, tiled=True)  11.9 us
    dot_general x1, matrix products, experts_layer(): up_sum = jnp.dot(portion, w_up, preferred_element_type=jnp.float32)  7.36 us
    all_to_all x1, starting transfers between devices, experts_layer(): lax.all_to_all(summed, 'ep', split_axis=0, concat_axis=0, tiled=True)  5.49 us
  transfers between devices with their start and end apart: 5, of which 3 were waited for; matrix products, arithmetic and copies ran while one was open for 23% of the time, Pallas kernels for 0%

profile of v1, /device:TPU:0, one launch (start us, length us, event | category | flops | bytes accessed | tf_op | source)
XLA Modules:
  0.0 190.2 jit_solution(14634247104931802326)
XLA Ops:
  11.0 2.4 %scatter_custom_fusion = s32[640]{0:T(1024)S(1)} fusion(s32[512]{0:T(512)S(1)} %bitcast.127, s32[512]{0:T(512)S(1)} %add_select_fusion, s32[]{:T(128)} %constant.68.clone.1), kind=kCustom, calls=%fused_computation.82 | custom fusion | bytes 2564 | tf_op jit(solution)/shard_map/scatter | solution.py:112
  13.5 1.5 fusion.9
  15.0 1.5 fusion.11
  16.5 4.1 %gather_fusion = bf16[640,2048]{1,0:T(8,128)(2,1)} fusion(bf16[256,2048]{1,0:T(8,128)(2,1)S(1)} %fusion.11, s32[1024]{0:T(1024)S(1)} %pad_clamp_fusion.1), kind=kCustom, calls=%fused_computation | custom fusion | bytes 5245440 | tf_op jit(solution)/shard_map/gather | solution.py:119
  20.6 3.8 %scatter_custom_fusion.1 = bf16[640]{0:T(1024)(128)(2,1)S(1)} fusion(s32[512]{0:T(512)S(1)} %bitcast.128, bf16[512]{0:T(512)(128)(2,1)S(1)} %broadcast.119, bf16[]{:T(256)} %constant.79.clone.1), kind=kCustom, calls=%fused_computation.87 | custom fusion | bytes 1282 | tf_op jit(solution)/shard_map/scatter | solution.py:117
  24.4 1.3 dynamic-slice_multiply_fusion
  25.7 24.9 %all_to_all.24 = bf16[8,80,512]{2,1,0:T(8,128)(2,1)} all-to-all(bf16[8,80,512]{2,1,0:T(8,128)(2,1)S(1)} %bitcast.115), channel_id=1, replica_groups=mesh['ep'=8,'tp'=4] {'ep'}, dimensions={0} | all-to-all | bytes 1310720 | tf_op jit(solution)/shard_map/all_to_all | solution.py:125
  53.9 2.2 %copy.118 = f32[256,4,128]{2,1,0:T(4,128)} copy(f32[256,4,128]{0,2,1:T(8,128)} %bitcast.117) | data formatting | bytes 1048576 | tf_op jit(solution)/shard_map/reshape | solution.py:54
  58.8 2.8 %bitcast_multiply_fusion.2 = (f32[4,256,128]{2,0,1:T(4,128)}, f32[4,256,128]{2,0,1:T(4,128)S(1)}, f32[4,256,128]{2,0,1:T(4,128)S(1)}) fusion(f32[256,4,128]{2,1,0:T(4,128)} %copy.118, f32[4,128,256]{1,2,0:T(8,128)S(1)} %bitcast.113, f32[4,128]{1,0:T(4,128)S(1)} %get-tuple-element.60, f32[256,4,128]{2,1,0:T(4,128)} %copy.112), kind=kLoop, calls=%fused_computation.47 | loop fusion | flops 655360 | bytes 3147776 | tf_op jit(solution)/shard_map/mul | solution.py:61
  61.5 1.3 convolution_convert_fusion.1
  63.1 11.9 %all-gather.8.cloned.1.call-done = bf16[640,2048]{1,0:T(8,128)(2,1)} async-done(((bf16[640,512]{1,0:T(8,128)(2,1)}), bf16[640,2048]{1,0:T(8,128)(2,1)}) %all-gather.8.cloned.1.call-update) | async-done | bytes 2621456 | tf_op jit(solution)/shard_map/all_gather | solution.py:126
  75.0 7.4 %fusion.2 = f32[640,1024]{1,0:T(8,128)} fusion(bf16[640,2048]{1,0:T(8,128)(2,1)} %all-gather.8.cloned.1.call-done, bf16[1,2048,1024]{2,1,0:T(8,128)(2,1)} %param.30), kind=kOutput, calls=%fused_computation.8 | convolution fusion | flops 2684354560 | bytes 9437184 | tf_op jit(solution)/shard_map/dot_general | solution.py:128
  82.3 12.5 %fusion.6 = bf16[640,2048]{1,0:T(8,128)(2,1)} fusion(bf16[1,1024,2048]{2,1,0:T(8,128)(2,1)} %param.31, f32[640,1024]{1,0:T(8,128)} %fusion.2, bf16[640,2048]{1,0:T(8,128)(2,1)} %all-gather.8.cloned.1.call-done, bf16[1,2048,1024]{2,1,0:T(8,128)(2,1)} %param.29), kind=kOutput, calls=%fused_computation.12 | convolution fusion | flops 5373952000 | bytes 16252928 | tf_op jit(solution)/shard_map/dot_general | solution.py:130
  94.9 26.4 %all-gather = bf16[32,1,128]{2,1,0:T(2,128)(2,1)S(1)} all-gather(bf16[4,1,128]{2,1,0:T(2,128)(2,1)S(1)} %copy.123), channel_id=2, replica_groups=mesh['ep'=8,'tp'=4] {'ep'}, dimensions={0}, use_global_device_ids=true | all-gather | bytes 9216 | tf_op jit(solution)/shard_map/all_gather | solution.py:14
  121.6 3.0 %convolution_select_fusion = f32[4,256,256]{2,1,0:T(8,128)} fusion(f32[4,256,128]{2,0,1:T(4,128)} %get-tuple-element.57, pred[256,256]{1,0:T(8,128)(4,1)S(1)} %iota_compare_fusion, f32[4,256,128]{2,0,1:T(4,128)S(1)} %get-tuple-element.59), kind=kOutput, calls=%fused_computation.19 | convolution fusion | flops 402915328 | bytes 2162688 | tf_op jit(solution)/shard_map/htk,hsk->hts/dot_general | solution.py:60
  125.4 2.2 %multiply_reduce_fusion.1 = (f32[4,256]{1,0:T(4,128)S(1)}, f32[4,256,128]{1,2,0:T(8,128)S(1)}) fusion(f32[4,256,128]{1,2,0:T(8,128)S(1)} %fusion.36, f32[4,256,256]{2,1,0:T(8,128)} %convolution_select_fusion, bf16[256,512]{1,0:T(8,128)(2,1)} %param.19), kind=kOutput, calls=%fused_computation.54 | convolution fusion | flops 403045376 | bytes 2363392 | tf_op jit(solution)/shard_map/hts,hsv->htv/dot_general | solution.py:65
  128.6 25.1 %reduce-scatter.2.cloned.1.call-done = bf16[640,512]{1,0:T(8,128)(2,1)} async-done(((bf16[640,2048]{1,0:T(8,128)(2,1)}), bf16[640,512]{1,0:T(8,128)(2,1)}) %reduce-scatter.2.cloned.1.call-update) | async-done | bytes 655376 | tf_op jit(solution)/shard_map/reduce_scatter | solution.py:131
  153.7 5.5 %all-to-all-start.1 = ((bf16[8,80,512]{2,1,0:T(8,128)(2,1)}), bf16[8,80,512]{2,1,0:T(8,128)(2,1)S(1)}, u32[]{:S(2)}, u32[]{:S(2)}) async-start(bf16[8,80,512]{2,1,0:T(8,128)(2,1)} %bitcast.123), calls=%async_computation.2 | async-start | bytes 1310720 | tf_op jit(solution)/shard_map/all_to_all | solution.py:134
  159.3 13.1 %all-gather.6.cloned.1.call-done = bf16[4,256,512]{2,1,0:T(8,128)(2,1)} async-done(((bf16[1,256,512]{2,1,0:T(8,128)(2,1)}), bf16[4,256,512]{2,1,0:T(8,128)(2,1)}) %all-gather.6.cloned.1.call-update) | async-done | bytes 1048592 | tf_op jit(solution)/shard_map/all_gather | solution.py:87
  172.4 2.3 %copy.129 = bf16[4,256,512]{1,2,0:T(8,128)(2,1)} copy(bf16[4,256,512]{2,1,0:T(8,128)(2,1)} %all-gather.6.cloned.1.call-done) | data formatting | bytes 2097152 | tf_op jit(solution)/shard_map/all_gather | solution.py:87
  174.7 2.7 %convolution_convert_fusion = bf16[256,512]{1,0:T(8,128)(2,1)} fusion(bf16[256,2048]{0,1:T(8,128)(2,1)} %bitcast.122, bf16[2048,512]{1,0:T(8,128)(2,1)S(1)} %copy-done), kind=kOutput, calls=%fused_computation.21 | convolution fusion | flops 537001984 | bytes 3407872 | tf_op jit(solution)/shard_map/dot_general | solution.py:86
  177.3 2.6 %gather_fusion.1 = bf16[512,512]{1,0:T(8,128)(2,1)} fusion(bf16[640,512]{1,0:T(8,128)(2,1)S(1)} %bitcast.111, s32[1024]{0:T(1024)S(1)} %pad_clamp_fusion), kind=kCustom, calls=%fused_computation.1 | custom fusion | bytes 1050624 | tf_op jit(solution)/shard_map/gather | solution.py:135
  179.9 1.7 reshape.176
  181.6 2.1 %multiply_reduce_fusion = bf16[256,512]{1,0:T(8,128)(2,1)} fusion(f32[256,2,512]{2,1,0:T(2,128)S(1)} %reshape.176, f32[256,2]{1,0:T(8,128)S(1)} %copy.133), kind=kLoop, calls=%fused_computation.23 | loop fusion | flops 393216 | bytes 1312768 | tf_op jit(solution)/shard_map/reduce_sum | solution.py:136
  (71 shorter events, 12.2 us)
Async XLA Ops:
  7.2 167.5 %copy-start = (bf16[2048,512]{1,0:T(8,128)(2,1)S(1)}, bf16[2048,512]{1,0:T(8,128)(2,1)}, u32[]{:S(2)}) copy-start(bf16[2048,512]{1,0:T(8,128)(2,1)} %param.24) | copy-start | bytes 6291460
  7.2 67.8 %all-gather.8.cloned.1.call-start = ((), (), s32[]{:S(2)}) async-start(), calls=%async_computation.4 | async-start | bytes 3276800 | tf_op jit(solution)/shard_map/all_gather | solution.py:126
  20.6 30.0 %copy-start.2 = (bf16[256,512]{1,0:T(8,128)(2,1)S(1)}, bf16[256,512]{1,0:T(8,128)(2,1)}, u32[]{:S(2)}) copy-start(bf16[256,512]{1,0:T(8,128)(2,1)} %param.18) | copy-start | bytes 786436
  20.6 30.2 %copy-start.4 = (f32[512]{0:T(512)S(1)}, f32[512]{0:T(512)}, u32[]{:S(2)}) copy-start(f32[512]{0:T(512)} %param.22) | copy-start | bytes 6148
  20.6 30.2 %copy-start.5 = (f32[256,4]{0,1:T(4,128)S(1)}, f32[256,4]{0,1:T(4,128)}, u32[]{:S(2)}) copy-start(f32[256,4]{0,1:T(4,128)} %param.21) | copy-start | bytes 12292
  50.6 74.1 %all-gather.10.cloned.1.call-start = ((), (), s32[]{:S(2)}) async-start(), calls=%async_computation.6 | async-start | bytes 1179648 | tf_op jit(solution)/shard_map/all_gather | solution.py:14
  53.9 7.6 %copy-start.1 = (bf16[256,512]{1,0:T(8,128)(2,1)S(1)}, bf16[256,512]{1,0:T(8,128)(2,1)}, u32[]{:S(2)}) copy-start(bf16[256,512]{1,0:T(8,128)(2,1)} %param.19) | copy-start | bytes 786436
  62.9 90.8 %reduce-scatter.2.cloned.1.call-start = ((), (), s32[]{:S(2)}) async-start(), calls=%async_computation.5 | async-start | bytes 3276800 | tf_op jit(solution)/shard_map/reduce_scatter | solution.py:131
  94.8 26.5 %copy-start.3 = (bf16[256,512]{1,0:T(8,128)(2,1)S(1)}, bf16[256,512]{1,0:T(8,128)(2,1)}, u32[]{:S(2)}) copy-start(bf16[256,512]{1,0:T(8,128)(2,1)} %param.20) | copy-start | bytes 786436
  94.8 77.6 %all-gather.6.cloned.1.call-start = ((), (), s32[]{:S(2)}) async-start(), calls=%async_computation.3 | async-start | bytes 1310720 | tf_op jit(solution)/shard_map/all_gather | solution.py:87
  124.7 2.9 %copy-start.7 = (f32[128]{0:T(128)S(1)}, f32[128]{0:T(128)}, u32[]{:S(2)}) copy-start(f32[128]{0:T(128)} %param.23) | copy-start | bytes 1540
  125.4 33.8 %copy-start.6 = (f32[256,2]{0,1:T(2,128)S(1)}, f32[256,2]{0,1:T(2,128)}, u32[]{:S(2)}) copy-start(f32[256,2]{0,1:T(2,128)} %param.28) | copy-start | bytes 6148
  153.7 23.6 %all-to-all-start.1 = ((bf16[8,80,512]{2,1,0:T(8,128)(2,1)}), bf16[8,80,512]{2,1,0:T(8,128)(2,1)S(1)}, u32[]{:S(2)}, u32[]{:S(2)}) async-start(bf16[8,80,512]{2,1,0:T(8,128)(2,1)} %bitcast.123), calls=%async_computation.2 | async-start | bytes 1310720 | tf_op jit(solution)/shard_map/all_to_all | solution.py:134
Sparse Core Ops, SparseCore 0:
  50.7 24.2 all-gather.7
  77.7 40.3 all-gather.9
  120.5 33.0 reduce-scatter.1
  155.7 16.6 all-gather.5
